TPU v7x, 32 devices: a whole 2x2x4 slice. The times are simulated.
32 devices in a mesh: ep: 8 (over z, y), tp: 4 (over x, core).
Axes of the slice: x: 2, y: 2, z: 4, core: 2. Of those that a mesh axis runs over, the one named last changes fastest.
Arguments:
- tokens: bfloat16 [24, 2048], P('ep'), may hold values from -6 to 6
- mixer_gain: float32 [2048], replicated, may hold values from 0.1 to 1.9
- query_weight: bfloat16 [2048, 2048], P('ep', 'tp'), may hold values from -0.125 to 0.125
- key_cache: bfloat16 [24, 1024, 4, 128], P('ep', None, 'tp'), may hold values from -6 to 6
- value_cache: bfloat16 [24, 1024, 4, 128], P('ep', None, 'tp'), may hold values from -6 to 6
- seq_lengths: int32 [24], P('ep'), may hold values from 1 to 1024, as said below
- head_offset: float32 [16], P('tp'), may hold values from -8.5 to -3.5
- output_weight: bfloat16 [2048, 2048], P('tp', 'ep'), may hold values from -0.5 to 0.5
- expert_gain: float32 [2048], replicated, may hold values from 0.1 to 1.9
- expert_ids: int32 [24, 2], P('ep'), may hold values from 0 to 7, as said below
- route_weight: float32 [24, 2], P('ep'), may hold values from 0.2 to 1
- gate_weight: bfloat16 [8, 2048, 1024], P('ep', None, 'tp'), may hold values from -0.125 to 0.125
- up_weight: bfloat16 [8, 2048, 1024], P('ep', None, 'tp'), may hold values from -0.125 to 0.125
- down_weight: bfloat16 [8, 1024, 2048], P('ep', 'tp'), may hold values from -0.1875 to 0.1875
Outputs:
- layer_out: bfloat16 [24, 2048], P('ep', 'tp')
Inputs may be any that keep to these rules, and one draw needn't show every extreme that they name: `seq_lengths`: some sequence holds all 1024 positions. `expert_ids`: the 2 experts of a row are different and lie in one group of 4 consecutive expert numbers. Among the 3 rows of one index of ep no expert is named by more than 2 rows, and some expert by exactly 2.
All inputs are finite; a program needn't handle non-finite values.
Results may differ from a plain program's by a relative error of at most 0.012.
Values may be sent and summed in bfloat16 or wider, within the bound.
No kernel may reach another device: no remote copies, remote signals or barrier semaphores. Data moves between devices by JAX's collectives and lax.ppermute only.
A program may use at most 64 MiB of HBM per device.

v0:
```python
import jax
import jax.numpy as jnp
from jax import lax
from jax.sharding import PartitionSpec as P

EPG = 4
TOP = 2
BLK = 256


def rms_norm(values, gain):
    wide = values.astype(jnp.float32)
    scale = lax.rsqrt(jnp.mean(wide * wide, axis=-1, keepdims=True) + 1e-06)
    return (wide * scale * gain).astype(jnp.bfloat16)


def attend_cache(query, key_cache, value_cache, seq_lengths, head_offset):
    batch = query.shape[0]
    local_heads = head_offset.shape[0]
    kv_local = key_cache.shape[2]
    head_size = key_cache.shape[3]
    per_group = local_heads // kv_local
    grouped = query.reshape(batch, kv_local, per_group, head_size)
    offset = head_offset.reshape(1, kv_local, per_group, 1)
    scale = head_size ** (-0.5)
    longest = jnp.max(seq_lengths)
    block_count = (longest + BLK - 1) // BLK

    def step(turn, carry):
        total, later = carry
        start = (block_count - 1 - turn) * BLK
        keys = lax.dynamic_slice_in_dim(key_cache, start, BLK, 1)
        values = lax.dynamic_slice_in_dim(value_cache, start, BLK, 1)
        score = (
            jnp.einsum("bkgd,bskd->bkgs", grouped, keys, preferred_element_type=jnp.float32) * scale
            + offset
        )
        places = start + jnp.arange(BLK, dtype=jnp.int32)
        valid = (places[None, :] < seq_lengths[:, None])[:, None, None, :]
        log_take = jax.nn.log_sigmoid(score)
        log_pass = jnp.where(valid, jax.nn.log_sigmoid(-score), 0.0)
        inside = lax.cumsum(log_pass, axis=3, reverse=True) - log_pass + later[..., None]
        weight = jnp.where(valid, jnp.exp(log_take + inside), 0.0).astype(jnp.bfloat16)
        total = total + jnp.einsum(
            "bkgs,bskd->bkgd", weight, values, preferred_element_type=jnp.float32
        )
        return (total, later + jnp.sum(log_pass, axis=3))

    start_total = jnp.zeros((batch, kv_local, per_group, head_size), jnp.float32)
    start_later = jnp.zeros((batch, kv_local, per_group), jnp.float32)
    total, later = lax.fori_loop(0, block_count, step, (start_total, start_later))
    return total.reshape(batch, local_heads * head_size).astype(jnp.bfloat16)


def expert_hidden(rows, gate_weight, up_weight):
    gate = jnp.dot(rows, gate_weight[0], preferred_element_type=jnp.float32)
    upward = jnp.dot(rows, up_weight[0], preferred_element_type=jnp.float32)
    return (jax.nn.silu(gate) * upward).astype(jnp.bfloat16)


def local(
    tokens,
    mixer_gain,
    query_weight,
    key_cache,
    value_cache,
    seq_lengths,
    head_offset,
    output_weight,
    expert_gain,
    expert_ids,
    route_weight,
    gate_weight,
    up_weight,
    down_weight,
):
    ep_count = lax.axis_size("ep")
    batch = tokens.shape[0]
    normed = rms_norm(tokens, mixer_gain)
    feature_rows = lax.all_to_all(normed, "ep", split_axis=1, concat_axis=0, tiled=True)
    query = lax.psum_scatter(
        jnp.dot(feature_rows, query_weight, preferred_element_type=jnp.float32),
        "ep",
        scatter_dimension=0,
        tiled=True,
    )
    query = query.astype(jnp.bfloat16)
    mixed = attend_cache(query, key_cache, value_cache, seq_lengths, head_offset)
    partial_value = jnp.dot(
        lax.all_gather(mixed, "ep", axis=0, tiled=True),
        output_weight,
        preferred_element_type=jnp.float32,
    ).astype(jnp.bfloat16)
    summed = lax.psum(partial_value, "tp").astype(jnp.float32)
    attention = lax.all_to_all(summed, "ep", split_axis=0, concat_axis=1, tiled=True)
    resid = (tokens.astype(jnp.float32) + attention).astype(jnp.bfloat16)
    normed2 = rms_norm(resid, expert_gain)
    group_total = ep_count // EPG
    slot_count = max(2, (batch + group_total - 1) // group_total)
    pair_count = batch * TOP
    pair_ids = expert_ids.reshape(pair_count)
    order = jnp.arange(pair_count, dtype=jnp.int32)
    earlier = (order[None, :] < order[:, None]) & (pair_ids[:, None] == pair_ids[None, :])
    slot_index = jnp.sum(earlier.astype(jnp.int32), axis=1)
    dest_slot = pair_ids * slot_count + slot_index
    places = jnp.arange(ep_count * slot_count, dtype=jnp.int32)
    dispatch = (places[:, None] == dest_slot[None, :]).astype(jnp.bfloat16)
    pair_rows = jnp.repeat(normed2, TOP, axis=0)
    outgoing = jnp.dot(dispatch, pair_rows, preferred_element_type=jnp.float32).astype(jnp.bfloat16)
    outgoing = outgoing.reshape(ep_count, slot_count, normed2.shape[1])
    received = lax.all_to_all(outgoing, "ep", split_axis=0, concat_axis=0, tiled=True)
    count = received.shape[1]
    flat_rows = received.reshape(ep_count * count, received.shape[2])
    hidden = expert_hidden(flat_rows, gate_weight, up_weight)
    term = jnp.dot(hidden, down_weight[0], preferred_element_type=jnp.float32)
    reduced = lax.psum_scatter(term.astype(jnp.bfloat16), "tp", scatter_dimension=1, tiled=True)
    results = reduced.reshape(ep_count, count, reduced.shape[1])
    returned = lax.all_to_all(results, "ep", split_axis=0, concat_axis=0, tiled=True)
    columns = returned.shape[2]
    picked = jnp.dot(
        dispatch.T,
        returned.reshape(ep_count * slot_count, columns),
        preferred_element_type=jnp.float32,
    )
    weighted = picked.reshape(batch, TOP, columns) * route_weight[:, :, None]
    mixture = jnp.sum(weighted, axis=1)
    slice_width = mixture.shape[1]
    column_start = lax.axis_index("tp") * slice_width
    resid_slice = lax.dynamic_slice_in_dim(resid, column_start, slice_width, 1)
    return (resid_slice.astype(jnp.float32) + mixture).astype(jnp.bfloat16)


def solution(mesh):
    in_specs = (
        P("ep", None),
        P(),
        P("ep", "tp"),
        P("ep", None, "tp", None),
        P("ep", None, "tp", None),
        P("ep"),
        P("tp"),
        P("tp", "ep"),
        P(),
        P("ep", None),
        P("ep", None),
        P("ep", None, "tp"),
        P("ep", None, "tp"),
        P("ep", "tp", None),
    )
    out_specs = P("ep", "tp")
    return jax.shard_map(local, mesh=mesh, in_specs=in_specs, out_specs=out_specs, check_vma=False)
```

profile of v0, /device:TPU:0, one launch (start us, length us, event | category | flops | bytes accessed | tf_op | source)
XLA Modules:
  0.0 231.2 jit_solution(9833385639679030872)
XLA Ops:
  6.5 0.9 fusion.32
  7.5 1.4 fusion.34
  8.9 7.4 %all-to-all-start = ((bf16[3,8,256]{2,0,1:T(4,128)(2,1)}), bf16[3,8,256]{2,0,1:T(4,128)(2,1)S(1)}, u32[]{:S(2)}, u32[]{:S(2)}) async-start(bf16[3,8,256]{2,0,1:T(4,128)(2,1)} %bitcast.12), calls=%async_computation | async-start | bytes 32768 | tf_op jit(solution)/shard_map/all_to_all | solution.py:80
  20.4 2.5 %all-to-all-done = bf16[3,8,256]{2,0,1:T(4,128)(2,1)S(1)} async-done(((bf16[3,8,256]{2,0,1:T(4,128)(2,1)}), bf16[3,8,256]{2,0,1:T(4,128)(2,1)S(1)}, u32[]{:S(2)}, u32[]{:S(2)}) %all-to-all-start) | async-done | bytes 12320 | tf_op jit(solution)/shard_map/all_to_all | solution.py:80
  22.9 1.1 fusion.49
  24.0 35.5 %all-reduce = bf16[24,512]{1,0:T(8,128)(2,1)S(1)} all-reduce(f32[24,512]{1,0:T(8,128)S(1)} %fusion.49), channel_id=2, replica_groups=mesh['ep'=8,'tp'=4] {'ep'}, use_global_device_ids=true, to_apply=%region_2.0.clone | all-reduce | flops 12288 | bytes 73728
  60.3 36.0 %while.14 = (s32[]{:T(128)}, f32[3,1,4,128]{3,2,0,1:T(4,128)S(1)}, f32[3,1,4]{2,0,1:T(4,128)S(1)}, s32[]{:T(128)}, s32[]{:T(128)}, /*index=5*/s32[3]{0:T(128)S(1...) while((s32[]{:T(128)}, f32[3,1,4,128]{3,2,0,1:T(4,128)S(1)}, ...), condition=%wide.region_7.8_spmd, body=%wide.region_3.7_spmd.sunk | while | flops 2042411 | bytes 598647 | solution.py:51
  60.3 1.2 fusion.64
  61.6 15.1 %reduce-window.16 = f32[3,1,4,2,128]{4,3,2,1,0:T(2,128)S(1)} reduce-window(f32[3,1,4,2,128]{4,3,2,1,0:T(2,128)S(1)} %bitcast.80, f32[]{:T(128)} %constant.65.clone.1..sunk), window={size=1x1x1x1x128 pad=0_0x0_0x0_0x0_0x0_127}, to_apply=%region_4.4 | reduce-window | flops 390144 | bytes 24580 | tf_op jit(solution)/shard_map/reduce-window.4
  77.1 1.1 fusion.65
  78.4 1.2 fusion.64
  79.6 15.1 %reduce-window.16 = f32[3,1,4,2,128]{4,3,2,1,0:T(2,128)S(1)} reduce-window(f32[3,1,4,2,128]{4,3,2,1,0:T(2,128)S(1)} %bitcast.80, f32[]{:T(128)} %constant.65.clone.1..sunk), window={size=1x1x1x1x128 pad=0_0x0_0x0_0x0_0x0_127}, to_apply=%region_4.4 | reduce-window | flops 390144 | bytes 24580 | tf_op jit(solution)/shard_map/reduce-window.4
  95.1 1.1 fusion.65
  96.3 64.1 %all-gather = bf16[8,3,512]{2,1,0:T(4,128)(2,1)S(1)} all-gather(bf16[1,3,512]{2,1,0:T(4,128)(2,1)S(1)} %reshape.218), channel_id=1, replica_groups=mesh['ep'=8,'tp'=4] {'ep'}, dimensions={0}, use_global_device_ids=true | all-gather | bytes 27648 | tf_op jit(solution)/shard_map/all_gather | solution.py:90
  160.6 10.3 %psum.7 = bf16[8,3,256]{2,1,0:T(4,128)(2,1)S(1)} all-reduce(bf16[8,3,256]{2,1,0:T(4,128)(2,1)S(1)} %all_to_all.40), channel_id=1, replica_groups=mesh['ep'=8,'tp'=4] {'tp'}, use_global_device_ids=true, to_apply=%region_8.9 | all-reduce | flops 6144 | bytes 24576 | tf_op jit(solution)/shard_map/psum | solution.py:94
  171.5 3.3 %all-to-all-start.1 = ((f32[8,3,256]{2,1,0:T(4,128)}), f32[8,3,256]{2,1,0:T(4,128)S(1)}, u32[]{:S(2)}, u32[]{:S(2)}) async-start(f32[8,3,256]{2,1,0:T(4,128)} %all_to_all.41), calls=%async_computation.1 | async-start | bytes 65536 | tf_op jit(solution)/shard_map/all_to_all | solution.py:95
  174.9 6.6 %all-to-all-done.1 = f32[8,3,256]{2,1,0:T(4,128)S(1)} async-done(((f32[8,3,256]{2,1,0:T(4,128)}), f32[8,3,256]{2,1,0:T(4,128)S(1)}, u32[]{:S(2)}, u32[]{:S(2)}) %all-to-all-start.1) | async-done | bytes 24608 | tf_op jit(solution)/shard_map/all_to_all | solution.py:95
  181.9 9.3 %all_to_all.51 = bf16[8,2,2048]{2,1,0:T(2,128)(2,1)S(1)} all-to-all(bf16[8,2,2048]{2,1,0:T(2,128)(2,1)S(1)} %reshape.214), channel_id=1, replica_groups=mesh['ep'=8,'tp'=4] {'ep'}, dimensions={0} | all-to-all | bytes 131072 | tf_op jit(solution)/shard_map/all_to_all | solution.py:111
  191.5 1.4 convolution_convert_fusion
  192.9 17.3 %reduce-scatter.2.cloned.1.call-done = bf16[16,512]{1,0:T(8,128)(2,1)} async-done(((bf16[16,2048]{1,0:T(8,128)(2,1)}), bf16[16,512]{1,0:T(8,128)(2,1)}) %reduce-scatter.2.cloned.1.call-update) | async-done | bytes 16400 | tf_op jit(solution)/shard_map/reduce_scatter | solution.py:116
  210.2 1.3 reshape.216
  211.6 5.5 %all-to-all-start.3 = ((bf16[8,2,512]{2,1,0:T(2,128)(2,1)}), bf16[8,2,512]{2,1,0:T(2,128)(2,1)S(1)}, u32[]{:S(2)}, u32[]{:S(2)}) async-start(bf16[8,2,512]{2,1,0:T(2,128)(2,1)} %reshape.216), calls=%async_computation.4 | async-start | bytes 32768 | tf_op jit(solution)/shard_map/all_to_all | solution.py:118
  217.2 6.5 %all-to-all-done.3 = bf16[8,2,512]{2,1,0:T(2,128)(2,1)S(1)} async-done(((bf16[8,2,512]{2,1,0:T(2,128)(2,1)}), bf16[8,2,512]{2,1,0:T(2,128)(2,1)S(1)}, u32[]{:S(2)}, u32[]{:S(2)}) %all-to-all-start.3) | async-done | bytes 16416 | tf_op jit(solution)/shard_map/all_to_all | solution.py:118
  223.7 0.7 add_convert_fusion
  (77 shorter events, 6.3 us)
Async XLA Ops:
  6.5 185.0 %copy-start = (bf16[1,256,2048]{2,1,0:T(8,128)(2,1)S(1)}, bf16[1,256,2048]{2,1,0:T(8,128)(2,1)}, u32[]{:S(2)}) copy-start(bf16[1,256,2048]{2,1,0:T(8,128)(2,1)} %param.29) | copy-start | bytes 3145732
  6.5 1.0 copy-start.4
  8.9 7.4 %copy-start.7 = (s32[3,2]{0,1:T(2,128)S(1)}, s32[3,2]{0,1:T(2,128)}, u32[]{:S(2)}) copy-start(s32[3,2]{0,1:T(2,128)} %param.25) | copy-start | bytes 76
  8.9 14.0 %all-to-all-start = ((bf16[3,8,256]{2,0,1:T(4,128)(2,1)}), bf16[3,8,256]{2,0,1:T(4,128)(2,1)S(1)}, u32[]{:S(2)}, u32[]{:S(2)}) async-start(bf16[3,8,256]{2,0,1:T(4,128)(2,1)} %bitcast.12), calls=%async_computation | async-start | bytes 32768 | tf_op jit(solution)/shard_map/all_to_all | solution.py:80
  16.5 0.7 copy-start.5
  18.5 0.7 copy-start.10
  59.6 0.7 copy-start.9
  60.3 100.2 %copy-start.3 = (bf16[512,256]{1,0:T(8,128)(2,1)S(1)}, bf16[512,256]{1,0:T(8,128)(2,1)}, u32[]{:S(2)}) copy-start(bf16[512,256]{1,0:T(8,128)(2,1)} %param.23) | copy-start | bytes 786436
  60.3 121.3 %copy-start.6 = (f32[2048]{0:T(1024)S(1)}, f32[2048]{0:T(1024)}, u32[]{:S(2)}) copy-start(f32[2048]{0:T(1024)} %param.24) | copy-start | bytes 24580
  96.3 94.9 %copy-start.1 = (bf16[1,2048,256]{2,1,0:T(8,128)(2,1)S(1)}, bf16[1,2048,256]{2,1,0:T(8,128)(2,1)}, u32[]{:S(2)}) copy-start(bf16[1,2048,256]{2,1,0:T(8,128)(2,1)} %param.27) | copy-start | bytes 3145732
  160.6 30.9 %copy-start.2 = (bf16[1,2048,256]{2,1,0:T(8,128)(2,1)S(1)}, bf16[1,2048,256]{2,1,0:T(8,128)(2,1)}, u32[]{:S(2)}) copy-start(bf16[1,2048,256]{2,1,0:T(8,128)(2,1)} %param.28) | copy-start | bytes 3145732
  171.5 10.0 %all-to-all-start.1 = ((f32[8,3,256]{2,1,0:T(4,128)}), f32[8,3,256]{2,1,0:T(4,128)S(1)}, u32[]{:S(2)}, u32[]{:S(2)}) async-start(f32[8,3,256]{2,1,0:T(4,128)} %all_to_all.41), calls=%async_computation.1 | async-start | bytes 65536 | tf_op jit(solution)/shard_map/all_to_all | solution.py:95
  174.8 35.4 %reduce-scatter.2.cloned.1.call-start = ((), (), s32[]{:S(2)}) async-start(), calls=%async_computation.5 | async-start | bytes 81920 | tf_op jit(solution)/shard_map/reduce_scatter | solution.py:116
  211.6 12.1 %all-to-all-start.3 = ((bf16[8,2,512]{2,1,0:T(2,128)(2,1)}), bf16[8,2,512]{2,1,0:T(2,128)(2,1)S(1)}, u32[]{:S(2)}, u32[]{:S(2)}) async-start(bf16[8,2,512]{2,1,0:T(2,128)(2,1)} %reshape.216), calls=%async_computation.4 | async-start | bytes 32768 | tf_op jit(solution)/shard_map/all_to_all | solution.py:118
  217.2 6.5 %copy-start.8 = (f32[3,2]{0,1:T(2,128)S(1)}, f32[3,2]{0,1:T(2,128)}, u32[]{:S(2)}) copy-start(f32[3,2]{0,1:T(2,128)} %param.26) | copy-start | bytes 76
Sparse Core Ops, SparseCore 0:
  193.0 17.1 reduce-scatter.1
where the time goes:
time: 231 us
  blocking collectives  119 us (52%)
  other arithmetic  35.2 us (15%)
  waiting for transfers between devices  32.9 us (14%)
  starting transfers between devices  16.3 us (7%)
  between operations  14.9 us (6%)
  matrix products  7.79 us (3%)
  local copies, waits for them, and re-layouts  4.99 us (2%)
    all_gather x1, blocking collectives, local(): lax.all_gather(mixed, 'ep', axis=0, tiled=True)  64.1 us
    unnamed x1, blocking collectives  35.5 us
    another operation x4, other arithmetic  30.3 us
    reduce_scatter x1, waiting for transfers between devices, local(): lax.psum_scatter(term.astype(jnp.bfloat16), 'tp', scatter_dimension=1, ti...  17.3 us
    psum x1, blocking collectives, local(): summed = lax.psum(partial_value, 'tp').astype(jnp.float32)  10.3 us
    all_to_all x1, blocking collectives, local(): lax.all_to_all(outgoing, 'ep', split_axis=0, concat_axis=0, tiled=True)  9.29 us
    all_to_all x1, starting transfers between devices, local(): lax.all_to_all(normed, 'ep', split_axis=1, concat_axis=0, tiled=True)  7.44 us
    all_to_all x1, waiting for transfers between devices, local(): lax.all_to_all(summed, 'ep', split_axis=0, concat_axis=1, tiled=True)  6.56 us
  transfers between devices with their start and end apart: 4, of which 4 were waited for; matrix products, arithmetic and copies ran while one was open for 1% of the time, Pallas kernels for 0%

commit v1 on v0

v1 whole, which is shorter than its diff:
```python
import functools

import jax
import jax.numpy as jnp
from jax import lax
from jax.experimental import pallas as pl
from jax.experimental.pallas import tpu as pltpu
from jax.sharding import PartitionSpec as P

LANES = 128


def rms_norm(values, gain):
    wide = values.astype(jnp.float32)
    scale = lax.rsqrt(jnp.mean(wide * wide, axis=-1, keepdims=True) + 1e-06)
    return (wide * scale * gain).astype(jnp.bfloat16)


def attend_body(length_ref, offset_ref, part_ref, key_ref, value_ref, out_ref):
    batch, places, head_size = key_ref.shape
    heads = offset_ref.shape[1]
    rows = -(-batch * heads // 8) * 8
    query = jnp.sum(part_ref[...], axis=0).astype(jnp.bfloat16)
    scale = head_size ** (-0.5)
    scores, lengths, offsets = [], [], []
    for b in range(batch):
        one = jnp.concatenate(
            [query[b : b + 1, h * head_size : (h + 1) * head_size] for h in range(heads)], axis=0
        )
        scores.append(
            lax.dot_general(
                one, key_ref[b], (((1,), (1,)), ((), ())), preferred_element_type=jnp.float32
            )
        )
        lengths.append(jnp.full((heads, places), length_ref[b], jnp.int32))
        for h in range(heads):
            offsets.append(jnp.full((1, places), offset_ref[0, h], jnp.float32))
    extra = rows - batch * heads
    if extra:
        scores.append(jnp.zeros((extra, places), jnp.float32))
        lengths.append(jnp.zeros((extra, places), jnp.int32))
        offsets.append(jnp.zeros((extra, places), jnp.float32))
    score = jnp.concatenate(scores, axis=0) * scale + jnp.concatenate(offsets, axis=0)
    valid = lax.broadcasted_iota(jnp.int32, (rows, places), 1) < jnp.concatenate(lengths, axis=0)
    soft = jnp.log1p(jnp.exp(-jnp.abs(score)))
    log_take = jnp.minimum(score, 0.0) - soft
    log_pass = jnp.where(valid, jnp.minimum(-score, 0.0) - soft, 0.0)
    chunks = places // LANES
    stacked = jnp.concatenate(
        [log_pass[:, c * LANES : (c + 1) * LANES] for c in range(chunks)], axis=0
    )
    high = stacked.astype(jnp.bfloat16)
    rest = stacked - high.astype(jnp.float32)
    middle = rest.astype(jnp.bfloat16)
    low = (rest - middle.astype(jnp.float32)).astype(jnp.bfloat16)
    source = lax.broadcasted_iota(jnp.int32, (LANES, LANES), 0)
    target = lax.broadcasted_iota(jnp.int32, (LANES, LANES), 1)
    after = (source > target).astype(jnp.bfloat16)
    dot = functools.partial(jnp.dot, preferred_element_type=jnp.float32)
    inside = dot(low, after) + dot(middle, after) + dot(high, after)
    totals = jnp.sum(stacked, axis=1, keepdims=True)
    later = jnp.zeros((rows, 1), jnp.float32)
    pieces = [None] * chunks
    for c in reversed(range(chunks)):
        pieces[c] = inside[c * rows : (c + 1) * rows] + later
        later = later + totals[c * rows : (c + 1) * rows]
    weight = jnp.where(valid, jnp.exp(log_take + jnp.concatenate(pieces, axis=1)), 0.0)
    weight = weight.astype(jnp.bfloat16)
    for b in range(batch):
        mixed = dot(weight, value_ref[b]).astype(jnp.bfloat16)
        for h in range(heads):
            out_ref[b : b + 1, h * head_size : (h + 1) * head_size] = mixed[
                b * heads + h : b * heads + h + 1
            ]


def attend(parts, keys, values, lengths, offset):
    batch, _, head_size = keys.shape
    width = parts.shape[2]
    vmem = pl.BlockSpec(memory_space=pltpu.VMEM)
    smem = pl.BlockSpec(memory_space=pltpu.SMEM)
    return pl.pallas_call(
        attend_body,
        out_shape=jax.ShapeDtypeStruct((batch, width), jnp.bfloat16),
        in_specs=[smem, smem, vmem, vmem, vmem],
        out_specs=vmem,
        name="attend",
    )(lengths, offset.reshape(1, -1), parts, keys, values)


def spread(block, axes, count):
    wide = jnp.broadcast_to(block[None], (count,) + block.shape)
    return lax.all_to_all(wide, axes, split_axis=0, concat_axis=0, tiled=True)


def local(
    tokens,
    mixer_gain,
    query_weight,
    key_cache,
    value_cache,
    seq_lengths,
    head_offset,
    output_weight,
    expert_gain,
    expert_ids,
    route_weight,
    gate_weight,
    up_weight,
    down_weight,
):
    ep_count = lax.axis_size("ep")
    tp_count = lax.axis_size("tp")
    ep_index = lax.axis_index("ep")
    tp_index = lax.axis_index("tp")
    batch, width = tokens.shape
    total = ep_count * batch
    both = ("ep", "tp")
    columns = output_weight.shape[1]
    out_weight = lax.all_gather(output_weight, "tp", axis=0)

    all_tokens = spread(tokens, "ep", ep_count).reshape(total, width)
    normed = rms_norm(all_tokens, mixer_gain)
    feature_count = query_weight.shape[0]
    features = lax.dynamic_slice_in_dim(normed, ep_index * feature_count, feature_count, 1)
    partial_query = jnp.dot(features, query_weight, preferred_element_type=jnp.float32)
    parts = lax.all_to_all(partial_query, "ep", split_axis=0, concat_axis=0, tiled=True)
    parts = parts.reshape(ep_count, batch, parts.shape[1])

    batch_places = key_cache.shape[:2]
    keys = key_cache.reshape(*batch_places, -1)
    values = value_cache.reshape(*batch_places, -1)
    mixed = attend(parts, keys, values, seq_lengths, head_offset)

    spread_mixed = spread(mixed, both, ep_count * tp_count)
    spread_mixed = spread_mixed.reshape(ep_count, tp_count, batch, -1)
    token_columns = lax.dynamic_slice_in_dim(all_tokens, ep_index * columns, columns, 1)
    summed = token_columns.astype(jnp.float32)
    for quarter in range(tp_count):
        rows = spread_mixed[:, quarter].reshape(total, -1)
        part = jnp.dot(rows, out_weight[quarter], preferred_element_type=jnp.float32)
        summed = summed + part.astype(jnp.bfloat16).astype(jnp.float32)
    resid_columns = summed.astype(jnp.bfloat16)
    resid = spread(resid_columns, "ep", ep_count)
    resid = resid.reshape(ep_count, total, columns).transpose(1, 0, 2).reshape(total, width)

    normed2 = rms_norm(resid, expert_gain)
    gate = jnp.dot(normed2, gate_weight[0], preferred_element_type=jnp.float32)
    upward = jnp.dot(normed2, up_weight[0], preferred_element_type=jnp.float32)
    hidden = (jax.nn.silu(gate) * upward).astype(jnp.bfloat16)
    term = jnp.dot(hidden, down_weight[0], preferred_element_type=jnp.float32).astype(jnp.bfloat16)
    slice_width = width // tp_count
    outgoing = term.reshape(ep_count, batch, tp_count, slice_width).transpose(0, 2, 1, 3)
    outgoing = outgoing.reshape(ep_count * tp_count, batch, slice_width)
    returned = lax.all_to_all(outgoing, both, split_axis=0, concat_axis=0, tiled=True)
    returned = returned.reshape(ep_count, tp_count, batch, slice_width)
    expert_out = jnp.sum(returned.astype(jnp.float32), axis=1).astype(jnp.bfloat16)
    numbers = jnp.arange(ep_count, dtype=jnp.int32)[:, None, None]
    share = jnp.sum(jnp.where(expert_ids[None] == numbers, route_weight[None], 0.0), axis=2)
    mixture = jnp.sum(expert_out.astype(jnp.float32) * share[:, :, None], axis=0)
    own = lax.dynamic_slice(
        resid, (ep_index * batch, tp_index * slice_width), (batch, slice_width)
    )
    return (own.astype(jnp.float32) + mixture).astype(jnp.bfloat16)


def solution(mesh):
    in_specs = (
        P("ep", None),
        P(),
        P("ep", "tp"),
        P("ep", None, "tp", None),
        P("ep", None, "tp", None),
        P("ep"),
        P("tp"),
        P("tp", "ep"),
        P(),
        P("ep", None),
        P("ep", None),
        P("ep", None, "tp"),
        P("ep", None, "tp"),
        P("ep", "tp", None),
    )
    out_specs = P("ep", "tp")
    return jax.shard_map(local, mesh=mesh, in_specs=in_specs, out_specs=out_specs, check_vma=False)
```

time: 231 us -> 83.8 us (0.36)
  blocking collectives: 119 us -> 20.1 us
  other arithmetic: 35.2 us -> 1.33 us
  waiting for transfers between devices: 32.9 us -> 21 us
  starting transfers between devices: 16.3 us -> 13.2 us
  Pallas kernels: 0 us -> 2.71 us
    all_gather x1 -> x0, blocking collectives: 64.1 us -> none  [local(): lax.all_gather(mixed, 'ep', axis=0, tiled=True)]
    unnamed x1 -> x0, blocking collectives: 35.5 us -> none
    another operation x4 -> x0, other arithmetic: 30.3 us -> none
    reduce_scatter x1 -> x0, waiting for transfers between devices: 17.3 us -> none  [local(): lax.psum_scatter(term.astype(jnp.bfloat16), 'tp', scatter_dimension=1, ti...]
    all_to_all x1 -> x2, blocking collectives: 9.29 us -> 20.1 us  [the longest x1 10.1 us: spread(): return lax.all_to_all(wide, axes, split_axis=0, concat_axis=0, tiled=True)]
    psum x1 -> x0, blocking collectives: 10.3 us -> none  [local(): summed = lax.psum(partial_value, 'tp').astype(jnp.float32)]
    all_to_all x3, waiting for transfers between devices: 15.5 us -> 20.2 us  [the longest x2 13.6 us: spread(): return lax.all_to_all(wide, axes, split_axis=0, concat_axis=0, tiled=True)]
    all_to_all x3, starting transfers between devices: 16.3 us -> 13.2 us  [the longest x2 10.7 us: spread(): return lax.all_to_all(wide, axes, split_axis=0, concat_axis=0, tiled=True)]
  transfers between devices with their start and end apart: 4 -> 4, of which waited for: 4 -> 3; matrix products, arithmetic and copies ran while one was open for 1% -> 4% of each run, Pallas kernels for 0% -> 3%
where the time goes in v1:
time: 83.8 us; the launch traced here: 83.2 us
  waiting for transfers between devices  21 us (25%)
  blocking collectives  20.1 us (24%)
  between operations  13.6 us (16%)
  starting transfers between devices  13.2 us (16%)
  matrix products  5.68 us (7%)
  local copies, waits for them, and re-layouts  5.56 us (7%)
  Pallas kernels  2.71 us (3%)
  other arithmetic  1.33 us (2%)
    all_to_all x2, waiting for transfers between devices, spread(): return lax.all_to_all(wide, axes, split_axis=0, concat_axis=0, tiled=True)  13.6 us
    all_to_all x2, starting transfers between devices, spread(): return lax.all_to_all(wide, axes, split_axis=0, concat_axis=0, tiled=True)  10.7 us
    all_to_all x1, blocking collectives, spread(): return lax.all_to_all(wide, axes, split_axis=0, concat_axis=0, tiled=True)  10.1 us
    all_to_all x1, blocking collectives, local(): lax.all_to_all(partial_query, 'ep', split_axis=0, concat_axis=0, tiled=True)  9.98 us
    all_to_all x1, waiting for transfers between devices, local(): lax.all_to_all(outgoing, both, split_axis=0, concat_axis=0, tiled=True)  6.64 us
    dot_general x4, matrix products, local(): jnp.dot(rows, out_weight[quarter], preferred_element_type=jnp.float32)  4.51 us
    pallas_call x1, Pallas kernels, attend(): pl.pallas_call(attend_body, out_shape=jax.ShapeDtypeStruct((batch, width)...  2.71 us
    all_to_all x1, starting transfers between devices, local(): lax.all_to_all(outgoing, both, split_axis=0, concat_axis=0, tiled=True)  2.56 us
  transfers between devices with their start and end apart: 4, of which 3 were waited for; matrix products, arithmetic and copies ran while one was open for 4% of the time, Pallas kernels for 3%

profile of v1, /device:TPU:0, one launch (start us, length us, event | category | flops | bytes accessed | tf_op | source)
XLA Modules:
  0.0 83.2 jit_solution(11923788218284236738)
XLA Ops:
  6.5 0.7 all-gather.3.cloned.1.call-update
  7.3 0.7 broadcast_in_dim.14
  8.0 7.3 %all-to-all-start = ((bf16[8,3,2048]{2,1,0:T(4,128)(2,1)}), bf16[8,3,2048]{2,1,0:T(4,128)(2,1)S(1)}, u32[]{:S(2)}, u32[]{:S(2)}) async-start(bf16[8,3,2048]{2,1,0:T(4,128)(2,1)} %broadcast_in_dim.14), calls=%async_computation | async-start | bytes 262144 | tf_op jit(solution)/shard_map/all_to_all | solution.py:93
  15.3 0.8 dynamic-slice
  16.2 6.5 %all-to-all-done = bf16[8,3,2048]{2,1,0:T(4,128)(2,1)S(1)} async-done(((bf16[8,3,2048]{2,1,0:T(4,128)(2,1)}), bf16[8,3,2048]{2,1,0:T(4,128)(2,1)S(1)}, u32[]{:S(2)}, u32[]{:S(2)}) %all-to-all-start) | async-done | bytes 98336 | tf_op jit(solution)/shard_map/all_to_all | solution.py:93
  23.3 10.0 %all_to_all.29.part_ref = f32[8,3,512]{2,1,0:T(4,128)} all-to-all(f32[8,3,512]{2,1,0:T(4,128)S(1)} %all_to_all.19), channel_id=1, replica_groups=mesh['ep'=8,'tp'=4] {'ep'}, dimensions={0} | all-to-all | bytes 98304 | tf_op jit(solution)/shard_map/all_to_all | solution.py:127
  33.2 2.7 %attend.1 = bf16[3,512]{1,0:T(4,128)(2,1)} custom-call(s32[3]{0:T(128)} %length_ref.1, f32[1,4]{1,0:T(1,128)} %bitcast.42, f32[8,3,512]{2,1,0:T(4,128)} %all_to_all.29.part_ref, bf16[3,1024,128]{2,1,0:T(8,128)(2,1)} %bitcast.37, bf16[3,1024,128]{2,1,0:T(8,128)(2,1)} %bitcast.38), custom_call_target="tpu_custom_call" | custom-call | tf_op jit(solution)/shard_map/attend/pallas_call | solution.py:82
  35.9 0.7 broadcast_in_dim.15
  36.7 10.1 %all_to_all.30 = bf16[32,3,512]{2,1,0:T(4,128)(2,1)S(1)} all-to-all(bf16[32,3,512]{2,1,0:T(4,128)(2,1)S(1)} %broadcast_in_dim.15), channel_id=1, replica_groups=mesh['ep'=8,'tp'=4] {'ep','tp'}, dimensions={0} | all-to-all | bytes 196608 | tf_op jit(solution)/shard_map/all_to_all | solution.py:93
  47.0 1.2 %fusion.9 = f32[24,256]{1,0:T(8,128)S(1)} fusion(bf16[24,512]{1,0:T(8,128)(2,1)S(1)} %reshape_squeeze.12, bf16[2048,256]{1,0:T(8,128)(2,1)} %all-gather.3.cloned.1.call-done, bf16[24,2048]{1,0:T(8,128)(2,1)S(1)} %reshape.85, s32[]{:T(128)S(6)} %select_n.14), kind=kOutput, calls=%fused_computation.15 | convolution fusion | flops 6316032 | bytes 323588 | tf_op jit(solution)/shard_map/dot_general | solution.py:141
  48.2 1.1 %fusion.7 = f32[24,256]{1,0:T(8,128)S(1)} fusion(f32[24,256]{1,0:T(8,128)S(1)} %fusion.9, bf16[24,512]{1,0:T(8,128)(2,1)S(1)} %reshape_squeeze.13, bf16[2048,256]{1,0:T(8,128)(2,1)} %all-gather.3.cloned.1.call-done), kind=kOutput, calls=%fused_computation.12 | convolution fusion | flops 6309888 | bytes 335872 | tf_op jit(solution)/shard_map/dot_general | solution.py:141
  49.3 1.1 %fusion.5 = f32[24,256]{1,0:T(8,128)S(1)} fusion(f32[24,256]{1,0:T(8,128)S(1)} %fusion.7, bf16[24,512]{1,0:T(8,128)(2,1)S(1)} %reshape_squeeze.14, bf16[2048,256]{1,0:T(8,128)(2,1)} %all-gather.3.cloned.1.call-done), kind=kOutput, calls=%fused_computation.9 | convolution fusion | flops 6309888 | bytes 335872 | tf_op jit(solution)/shard_map/dot_general | solution.py:141
  50.4 1.1 %fusion.3 = bf16[24,256]{1,0:T(8,128)(2,1)S(1)} fusion(f32[24,256]{1,0:T(8,128)S(1)} %fusion.5, bf16[24,512]{1,0:T(8,128)(2,1)S(1)} %reshape_squeeze.15, bf16[2048,256]{1,0:T(8,128)(2,1)} %all-gather.3.cloned.1.call-done), kind=kOutput, calls=%fused_computation.6 | convolution fusion | flops 6316032 | bytes 323584 | tf_op jit(solution)/shard_map/dot_general | solution.py:141
  51.5 0.6 broadcast_in_dim.16
  52.2 3.4 %all-to-all-start.3 = ((bf16[8,24,256]{2,1,0:T(8,128)(2,1)}), bf16[8,24,256]{2,1,0:T(8,128)(2,1)S(1)}, u32[]{:S(2)}, u32[]{:S(2)}) async-start(bf16[8,24,256]{2,1,0:T(8,128)(2,1)} %broadcast_in_dim.16), calls=%async_computation.3 | async-start | bytes 196608 | tf_op jit(solution)/shard_map/all_to_all | solution.py:93
  55.6 7.1 %all-to-all-done.3 = bf16[8,24,256]{2,1,0:T(8,128)(2,1)S(1)} async-done(((bf16[8,24,256]{2,1,0:T(8,128)(2,1)}), bf16[8,24,256]{2,1,0:T(8,128)(2,1)S(1)}, u32[]{:S(2)}, u32[]{:S(2)}) %all-to-all-start.3) | async-done | bytes 98336 | tf_op jit(solution)/shard_map/all_to_all | solution.py:93
  62.9 0.2 fusion.13
  63.2 0.7 convolution_convert_fusion
  64.0 0.7 copy.62
  64.7 2.6 %all-to-all-start.4 = ((bf16[32,3,512]{2,1,0:T(4,128)(2,1)}), bf16[32,3,512]{2,1,0:T(4,128)(2,1)S(1)}, u32[]{:S(2)}, u32[]{:S(2)}) async-start(bf16[32,3,512]{2,1,0:T(4,128)(2,1)} %bitcast.9), calls=%async_computation.4 | async-start | bytes 262144 | tf_op jit(solution)/shard_map/all_to_all | solution.py:155
  67.3 0.7 copy-done.6
  68.0 0.6 copy-done.7
  68.8 6.6 %all-to-all-done.4 = bf16[32,3,512]{2,1,0:T(4,128)(2,1)S(1)} async-done(((bf16[32,3,512]{2,1,0:T(4,128)(2,1)}), bf16[32,3,512]{2,1,0:T(4,128)(2,1)S(1)}, u32[]{:S(2)}, u32[]{:S(2)}) %all-to-all-start.4) | async-done | bytes 98336 | tf_op jit(solution)/shard_map/all_to_all | solution.py:155
  75.6 0.7 add_convert_fusion
  (39 shorter events, 1.6 us)
Async XLA Ops:
  6.5 56.6 %copy-start = (bf16[1,256,2048]{2,1,0:T(8,128)(2,1)S(1)}, bf16[1,256,2048]{2,1,0:T(8,128)(2,1)}, u32[]{:S(2)}) copy-start(bf16[1,256,2048]{2,1,0:T(8,128)(2,1)} %param.27) | copy-start | bytes 3145732
  6.5 0.8 copy-start.4
  6.5 40.5 %all-gather.3.cloned.1.call-start = ((), (), s32[]{:S(2)}) async-start(), calls=%async_computation.5 | async-start | bytes 1310720 | tf_op jit(solution)/shard_map/all_gather | solution.py:120
  8.0 14.7 %all-to-all-start = ((bf16[8,3,2048]{2,1,0:T(4,128)(2,1)}), bf16[8,3,2048]{2,1,0:T(4,128)(2,1)S(1)}, u32[]{:S(2)}, u32[]{:S(2)}) async-start(bf16[8,3,2048]{2,1,0:T(4,128)(2,1)} %broadcast_in_dim.14), calls=%async_computation | async-start | bytes 262144 | tf_op jit(solution)/shard_map/all_to_all | solution.py:93
  15.3 7.7 %copy-start.3 = (bf16[256,512]{1,0:T(8,128)(2,1)S(1)}, bf16[256,512]{1,0:T(8,128)(2,1)}, u32[]{:S(2)}) copy-start(bf16[256,512]{1,0:T(8,128)(2,1)} %param.16) | copy-start | bytes 786436
  47.0 15.9 %copy-start.1 = (bf16[1,2048,256]{2,1,0:T(8,128)(2,1)S(1)}, bf16[1,2048,256]{2,1,0:T(8,128)(2,1)}, u32[]{:S(2)}) copy-start(bf16[1,2048,256]{2,1,0:T(8,128)(2,1)} %param.25) | copy-start | bytes 3145732
  50.4 5.1 %copy-start.5 = (f32[2048]{0:T(1024)S(1)}, f32[2048]{0:T(1024)}, u32[]{:S(2)}) copy-start(f32[2048]{0:T(1024)} %param.22) | copy-start | bytes 24580
  51.5 11.6 %copy-start.2 = (bf16[1,2048,256]{2,1,0:T(8,128)(2,1)S(1)}, bf16[1,2048,256]{2,1,0:T(8,128)(2,1)}, u32[]{:S(2)}) copy-start(bf16[1,2048,256]{2,1,0:T(8,128)(2,1)} %param.26) | copy-start | bytes 3145732
  52.2 10.5 %all-to-all-start.3 = ((bf16[8,24,256]{2,1,0:T(8,128)(2,1)}), bf16[8,24,256]{2,1,0:T(8,128)(2,1)S(1)}, u32[]{:S(2)}, u32[]{:S(2)}) async-start(bf16[8,24,256]{2,1,0:T(8,128)(2,1)} %broadcast_in_dim.16), calls=%async_computation.3 | async-start | bytes 196608 | tf_op jit(solution)/shard_map/all_to_all | solution.py:93
  64.7 10.8 %all-to-all-start.4 = ((bf16[32,3,512]{2,1,0:T(4,128)(2,1)}), bf16[32,3,512]{2,1,0:T(4,128)(2,1)S(1)}, u32[]{:S(2)}, u32[]{:S(2)}) async-start(bf16[32,3,512]{2,1,0:T(4,128)(2,1)} %bitcast.9), calls=%async_computation.4 | async-start | bytes 262144 | tf_op jit(solution)/shard_map/all_to_all | solution.py:155
  67.3 0.7 copy-start.6
  68.0 0.7 copy-start.7
Sparse Core Ops, SparseCore 0:
  8.9 19.4 all-gather.2

commit v2 on v1

--- a/solution.py
+++ b/solution.py
@@ -16,11 +16,13 @@
     return (wide * scale * gain).astype(jnp.bfloat16)
 
 
-def attend_body(length_ref, offset_ref, part_ref, key_ref, value_ref, out_ref):
+def attend_body(length_ref, offset_ref, part_ref, token_ref, key_ref, value_ref, out_ref):
     batch, places, head_size = key_ref.shape
     heads = offset_ref.shape[1]
     rows = -(-batch * heads // 8) * 8
-    query = jnp.sum(part_ref[...], axis=0).astype(jnp.bfloat16)
+    wide = token_ref[...].astype(jnp.float32)
+    norm = lax.rsqrt(jnp.mean(wide * wide, axis=-1, keepdims=True) + 1e-06)
+    query = (jnp.sum(part_ref[...], axis=0) * norm).astype(jnp.bfloat16)
     scale = head_size ** (-0.5)
     scores, lengths, offsets = [], [], []
     for b in range(batch):
@@ -66,26 +68,28 @@
         later = later + totals[c * rows : (c + 1) * rows]
     weight = jnp.where(valid, jnp.exp(log_take + jnp.concatenate(pieces, axis=1)), 0.0)
     weight = weight.astype(jnp.bfloat16)
+    mixed_rows = []
     for b in range(batch):
-        mixed = dot(weight, value_ref[b]).astype(jnp.bfloat16)
-        for h in range(heads):
-            out_ref[b : b + 1, h * head_size : (h + 1) * head_size] = mixed[
-                b * heads + h : b * heads + h + 1
-            ]
+        mixed = dot(weight, value_ref[b])
+        mixed_rows.append(
+            jnp.concatenate([mixed[b * heads + h : b * heads + h + 1] for h in range(heads)], axis=1)
+        )
+    mixed = jnp.concatenate(mixed_rows, axis=0).astype(jnp.bfloat16)
+    for copy in range(out_ref.shape[0]):
+        out_ref[copy] = mixed
 
 
-def attend(parts, keys, values, lengths, offset):
-    batch, _, head_size = keys.shape
-    width = parts.shape[2]
+def attend(parts, tokens, keys, values, lengths, offset, copies):
+    batch = tokens.shape[0]
     vmem = pl.BlockSpec(memory_space=pltpu.VMEM)
     smem = pl.BlockSpec(memory_space=pltpu.SMEM)
     return pl.pallas_call(
         attend_body,
-        out_shape=jax.ShapeDtypeStruct((batch, width), jnp.bfloat16),
-        in_specs=[smem, smem, vmem, vmem, vmem],
+        out_shape=jax.ShapeDtypeStruct((copies, batch, parts.shape[2]), jnp.bfloat16),
+        in_specs=[smem, smem, vmem, vmem, vmem, vmem],
         out_specs=vmem,
         name="attend",
-    )(lengths, offset.reshape(1, -1), parts, keys, values)
+    )(lengths, offset.reshape(1, -1), parts, tokens, keys, values)
 
 
 def spread(block, axes, count):
@@ -117,12 +121,11 @@
     total = ep_count * batch
     both = ("ep", "tp")
     columns = output_weight.shape[1]
-    out_weight = lax.all_gather(output_weight, "tp", axis=0)
 
-    all_tokens = spread(tokens, "ep", ep_count).reshape(total, width)
-    normed = rms_norm(all_tokens, mixer_gain)
     feature_count = query_weight.shape[0]
-    features = lax.dynamic_slice_in_dim(normed, ep_index * feature_count, feature_count, 1)
+    raw = lax.all_to_all(tokens, "ep", split_axis=1, concat_axis=0, tiled=True)
+    gain = lax.dynamic_slice_in_dim(mixer_gain, ep_index * feature_count, feature_count, 0)
+    features = (raw.astype(jnp.float32) * gain).astype(jnp.bfloat16)
     partial_query = jnp.dot(features, query_weight, preferred_element_type=jnp.float32)
     parts = lax.all_to_all(partial_query, "ep", split_axis=0, concat_axis=0, tiled=True)
     parts = parts.reshape(ep_count, batch, parts.shape[1])
@@ -130,19 +133,15 @@
     batch_places = key_cache.shape[:2]
     keys = key_cache.reshape(*batch_places, -1)
     values = value_cache.reshape(*batch_places, -1)
-    mixed = attend(parts, keys, values, seq_lengths, head_offset)
-
-    spread_mixed = spread(mixed, both, ep_count * tp_count)
-    spread_mixed = spread_mixed.reshape(ep_count, tp_count, batch, -1)
-    token_columns = lax.dynamic_slice_in_dim(all_tokens, ep_index * columns, columns, 1)
-    summed = token_columns.astype(jnp.float32)
-    for quarter in range(tp_count):
-        rows = spread_mixed[:, quarter].reshape(total, -1)
-        part = jnp.dot(rows, out_weight[quarter], preferred_element_type=jnp.float32)
-        summed = summed + part.astype(jnp.bfloat16).astype(jnp.float32)
-    resid_columns = summed.astype(jnp.bfloat16)
-    resid = spread(resid_columns, "ep", ep_count)
-    resid = resid.reshape(ep_count, total, columns).transpose(1, 0, 2).reshape(total, width)
+    outward = attend(parts, tokens, keys, values, seq_lengths, head_offset, ep_count)
+    inward = lax.all_to_all(outward, "ep", split_axis=0, concat_axis=0, tiled=True)
+    heads_out = inward.reshape(total, -1)
+    part = jnp.dot(heads_out, output_weight, preferred_element_type=jnp.float32)
+    part = part + jnp.where(tp_index == 0, raw.astype(jnp.float32), 0.0)
+    terms = spread(part.astype(jnp.bfloat16), both, ep_count * tp_count)
+    terms = terms.reshape(ep_count, tp_count, total, columns)
+    resid = jnp.sum(terms.astype(jnp.float32), axis=1).astype(jnp.bfloat16)
+    resid = resid.transpose(1, 0, 2).reshape(total, width)
 
     normed2 = rms_norm(resid, expert_gain)
     gate = jnp.dot(normed2, gate_weight[0], preferred_element_type=jnp.float32)

time: 83.8 us -> 70.4 us (0.84)
  between operations: 13.6 us -> 0.14 us
  waiting for transfers between devices: 21 us -> 32.3 us
  blocking collectives: 20.1 us -> 9.96 us
  starting transfers between devices: 13.2 us -> 16.1 us
  matrix products: 5.68 us -> 3.45 us
  local copies, waits for them, and re-layouts: 5.56 us -> 3.87 us
    all_to_all x0 -> x2, waiting for transfers between devices: none -> 12.4 us  [the longest x1 6.6 us: local(): lax.all_to_all(outward, 'ep', split_axis=0, concat_axis=0, tiled=True)]
    all_to_all x0 -> x2, starting transfers between devices: none -> 10.8 us  [the longest x1 7.44 us: local(): raw = lax.all_to_all(tokens, 'ep', split_axis=1, concat_axis=0, tiled=True)]
    all_to_all x1 -> x0, blocking collectives: 10.1 us -> none  [spread(): return lax.all_to_all(wide, axes, split_axis=0, concat_axis=0, tiled=True)]
    all_to_all x2 -> x1, starting transfers between devices: 10.7 us -> 2.73 us  [spread(): return lax.all_to_all(wide, axes, split_axis=0, concat_axis=0, tiled=True)]
    dot_general x4 -> x1, matrix products: 4.51 us -> 0.15 us  [local(): part = jnp.dot(heads_out, output_weight, preferred_element_type=jnp.float32)]
    broadcast_in_dim x3 -> x1, local copies, waits for them, and re-layouts: 2.04 us -> 0.76 us  [spread(): wide = jnp.broadcast_to(block[None], (count,) + block.shape)]
    dot_general x1, matrix products: 0.73 us -> 1.96 us  [local(): jnp.dot(hidden, down_weight[0], preferred_element_type=jnp.float32)]
    dot_general x1, matrix products: 0.19 us -> 1.09 us  [local(): jnp.dot(features, query_weight, preferred_element_type=jnp.float32)]
  transfers between devices with their start and end apart: 4 -> 4, of which waited for: 3 -> 4; matrix products, arithmetic and copies ran while one was open for 4% -> 2% of each run, Pallas kernels for 3% -> 0%
where the time goes in v2:
time: 70.4 us; the launch traced here: 69.9 us
  waiting for transfers between devices  32.3 us (46%)
  starting transfers between devices  16.1 us (23%)
  blocking collectives  9.96 us (14%)
  local copies, waits for them, and re-layouts  3.87 us (5%)
  matrix products  3.45 us (5%)
  Pallas kernels  2.88 us (4%)
  other arithmetic  1.24 us (2%)
    all_to_all x1, waiting for transfers between devices, spread(): return lax.all_to_all(wide, axes, split_axis=0, concat_axis=0, tiled=True)  13.2 us
    all_to_all x1, blocking collectives, local(): lax.all_to_all(partial_query, 'ep', split_axis=0, concat_axis=0, tiled=True)  9.96 us
    all_to_all x1, starting transfers between devices, local(): raw = lax.all_to_all(tokens, 'ep', split_axis=1, concat_axis=0, tiled=True)  7.44 us
    all_to_all x1, waiting for transfers between devices, local(): lax.all_to_all(outgoing, both, split_axis=0, concat_axis=0, tiled=True)  6.65 us
    all_to_all x1, waiting for transfers between devices, local(): lax.all_to_all(outward, 'ep', split_axis=0, concat_axis=0, tiled=True)  6.6 us
    all_to_all x1, waiting for transfers between devices, local(): raw = lax.all_to_all(tokens, 'ep', split_axis=1, concat_axis=0, tiled=True)  5.82 us
    all_to_all x1, starting transfers between devices, local(): lax.all_to_all(outward, 'ep', split_axis=0, concat_axis=0, tiled=True)  3.33 us
    pallas_call x1, Pallas kernels, attend(): pl.pallas_call(attend_body, out_shape=jax.ShapeDtypeStruct((copies, batch...  2.88 us
  transfers between devices with their start and end apart: 4, of which 4 were waited for; matrix products, arithmetic and copies ran while one was open for 2% of the time, Pallas kernels for 0%

profile of v2, /device:TPU:0, one launch (start us, length us, event | category | flops | bytes accessed | tf_op | source)
XLA Modules:
  0.0 69.9 jit_solution(3215592700969926694)
XLA Ops:
  0.0 7.4 %all-to-all-start = ((bf16[3,8,256]{2,0,1:T(4,128)(2,1)}), bf16[3,8,256]{2,0,1:T(4,128)(2,1)S(1)}, u32[]{:S(2)}, u32[]{:S(2)}) async-start(bf16[3,8,256]{2,0,1:T(4,128)(2,1)} %bitcast.47), calls=%async_computation | async-start | bytes 32768 | tf_op jit(solution)/shard_map/all_to_all | solution.py:126
  7.4 0.8 %dynamic_slice.6 = f32[256]{0:T(256)S(1)} dynamic-slice(f32[2048]{0:T(1024)} %param.15, s32[]{:T(128)S(6)} %select_n.27), dynamic_slice_sizes={256} | dynamic-slice | bytes 2052 | tf_op jit(solution)/shard_map/dynamic_slice | solution.py:127
  8.2 5.8 %all-to-all-done = bf16[3,8,256]{2,0,1:T(4,128)(2,1)S(1)} async-done(((bf16[3,8,256]{2,0,1:T(4,128)(2,1)}), bf16[3,8,256]{2,0,1:T(4,128)(2,1)S(1)}, u32[]{:S(2)}, u32[]{:S(2)}) %all-to-all-start) | async-done | bytes 12320 | tf_op jit(solution)/shard_map/all_to_all | solution.py:126
  14.0 1.1 %fusion.7 = f32[8,3,512]{2,0,1:T(8,128)S(1)} fusion(bf16[256,512]{1,0:T(8,128)(2,1)} %param.16, bf16[8,3,256]{2,1,0:T(4,128)(2,1)S(1)} %get-tuple-element.5), kind=kOutput, calls=%fused_computation.10 | convolution fusion | flops 6291456 | bytes 323584 | tf_op jit(solution)/shard_map/dot_general | solution.py:129
  15.2 10.0 %all_to_all.34.part_ref = f32[8,3,512]{2,1,0:T(4,128)} all-to-all(f32[8,3,512]{2,1,0:T(4,128)S(1)} %copy.43), channel_id=1, replica_groups=mesh['ep'=8,'tp'=4] {'ep'}, dimensions={0} | all-to-all | bytes 98304 | tf_op jit(solution)/shard_map/all_to_all | solution.py:130
  25.1 2.9 %attend.1 = bf16[8,3,512]{2,1,0:T(4,128)(2,1)} custom-call(s32[3]{0:T(128)} %length_ref.1, f32[1,4]{1,0:T(1,128)} %bitcast.48, f32[8,3,512]{2,1,0:T(4,128)} %all_to_all.34.part_ref, bf16[3,2048]{1,0:T(4,128)(2,1)} %token_ref.1, bf16[3,1024,128]{2,1,0:T(8,128)(2,1)} %bitcast.43, bf16[3,1024,128]{2,1,0:T(8,128)(2,1)} %bitcast.44), custom_call_target="tpu_custom_call" | custom-call | tf_op jit(solution)/shard_map/attend/pallas_call | solution.py:86
  28.0 3.3 %all-to-all-start.2 = ((bf16[8,3,512]{2,1,0:T(4,128)(2,1)}), bf16[8,3,512]{2,1,0:T(4,128)(2,1)S(1)}, u32[]{:S(2)}, u32[]{:S(2)}) async-start(bf16[8,3,512]{2,1,0:T(4,128)(2,1)} %attend.1), calls=%async_computation.2 | async-start | bytes 65536 | tf_op jit(solution)/shard_map/all_to_all | solution.py:137
  31.4 6.6 %all-to-all-done.2 = bf16[8,3,512]{2,1,0:T(4,128)(2,1)S(1)} async-done(((bf16[8,3,512]{2,1,0:T(4,128)(2,1)}), bf16[8,3,512]{2,1,0:T(4,128)(2,1)S(1)}, u32[]{:S(2)}, u32[]{:S(2)}) %all-to-all-start.2) | async-done | bytes 24608 | tf_op jit(solution)/shard_map/all_to_all | solution.py:137
  38.0 0.2 fusion
  38.2 0.8 %broadcast_in_dim.15 = bf16[32,24,256]{2,1,0:T(8,128)(2,1)} broadcast(bf16[24,256]{1,0:T(8,128)(2,1)S(1)} %fusion), dimensions={1,2} | broadcast | bytes 405504 | tf_op jit(solution)/shard_map/broadcast_in_dim | solution.py:96
  39.0 2.7 %all-to-all-start.3 = ((bf16[32,24,256]{2,1,0:T(8,128)(2,1)}), bf16[32,24,256]{2,1,0:T(8,128)(2,1)S(1)}, u32[]{:S(2)}, u32[]{:S(2)}) async-start(bf16[32,24,256]{2,1,0:T(8,128)(2,1)} %broadcast_in_dim.15), calls=%async_computation.3 | async-start | bytes 786432 | tf_op jit(solution)/shard_map/all_to_all | solution.py:97
  41.7 13.2 %all-to-all-done.3 = bf16[32,24,256]{2,1,0:T(8,128)(2,1)S(1)} async-done(((bf16[32,24,256]{2,1,0:T(8,128)(2,1)}), bf16[32,24,256]{2,1,0:T(8,128)(2,1)S(1)}, u32[]{:S(2)}, u32[]{:S(2)}) %all-to-all-start.3) | async-done | bytes 393248 | tf_op jit(solution)/shard_map/all_to_all | solution.py:97
  55.0 0.1 fusion.9
  55.1 0.1 fusion.12
  55.3 0.2 fusion.5
  55.5 2.0 %convolution_convert_fusion = bf16[24,2048]{1,0:T(8,128)(2,1)S(1)} fusion(bf16[24,2048]{1,0:T(8,128)(2,1)S(1)} %bitcast.42, bf16[1,256,2048]{2,1,0:T(8,128)(2,1)S(1)} %copy-done, bf16[1,2048,256]{2,1,0:T(8,128)(2,1)} %param.26, f32[24,256]{1,0:T(8,128)S(1)} %fusion.5), kind=kOutput, calls=%fused_computation | convolution fusion | flops 50417664 | bytes 2318336 | tf_op jit(solution)/shard_map/dot_general | solution.py:150
  57.6 0.7 %copy.51 = bf16[8,4,3,512]{3,2,1,0:T(4,128)(2,1)} copy(bf16[8,4,3,512]{3,1,2,0:T(4,128)(2,1)S(1)} %bitcast.45) | data formatting | bytes 196608 | tf_op jit(solution)/shard_map/reshape | solution.py:153
  58.3 2.6 %all-to-all-start.4 = ((bf16[32,3,512]{2,1,0:T(4,128)(2,1)}), bf16[32,3,512]{2,1,0:T(4,128)(2,1)S(1)}, u32[]{:S(2)}, u32[]{:S(2)}) async-start(bf16[32,3,512]{2,1,0:T(4,128)(2,1)} %bitcast.13), calls=%async_computation.4 | async-start | bytes 262144 | tf_op jit(solution)/shard_map/all_to_all | solution.py:154
  60.8 0.7 copy-done.4
  61.6 0.6 copy-done.5
  62.3 0.1 fusion.23
  62.4 6.6 %all-to-all-done.4 = bf16[32,3,512]{2,1,0:T(4,128)(2,1)S(1)} async-done(((bf16[32,3,512]{2,1,0:T(4,128)(2,1)}), bf16[32,3,512]{2,1,0:T(4,128)(2,1)S(1)}, u32[]{:S(2)}, u32[]{:S(2)}) %all-to-all-start.4) | async-done | bytes 98336 | tf_op jit(solution)/shard_map/all_to_all | solution.py:154
  69.1 0.1 multiply_reduce_fusion
  69.2 0.7 add_convert_fusion
  (23 shorter events, 0.5 us)
Async XLA Ops:
  0.0 55.5 %copy-start = (bf16[1,256,2048]{2,1,0:T(8,128)(2,1)S(1)}, bf16[1,256,2048]{2,1,0:T(8,128)(2,1)}, u32[]{:S(2)}) copy-start(bf16[1,256,2048]{2,1,0:T(8,128)(2,1)} %param.27) | copy-start | bytes 3145732
  0.0 14.0 %all-to-all-start = ((bf16[3,8,256]{2,0,1:T(4,128)(2,1)}), bf16[3,8,256]{2,0,1:T(4,128)(2,1)S(1)}, u32[]{:S(2)}, u32[]{:S(2)}) async-start(bf16[3,8,256]{2,0,1:T(4,128)(2,1)} %bitcast.47), calls=%async_computation | async-start | bytes 32768 | tf_op jit(solution)/shard_map/all_to_all | solution.py:126
  25.1 12.9 %copy-start.2 = (bf16[512,256]{1,0:T(8,128)(2,1)S(1)}, bf16[512,256]{1,0:T(8,128)(2,1)}, u32[]{:S(2)}) copy-start(bf16[512,256]{1,0:T(8,128)(2,1)} %param.21) | copy-start | bytes 786436
  28.0 10.0 %all-to-all-start.2 = ((bf16[8,3,512]{2,1,0:T(4,128)(2,1)}), bf16[8,3,512]{2,1,0:T(4,128)(2,1)S(1)}, u32[]{:S(2)}, u32[]{:S(2)}) async-start(bf16[8,3,512]{2,1,0:T(4,128)(2,1)} %attend.1), calls=%async_computation.2 | async-start | bytes 65536 | tf_op jit(solution)/shard_map/all_to_all | solution.py:137
  38.2 17.1 %copy-start.1 = (bf16[1,2048,256]{2,1,0:T(8,128)(2,1)S(1)}, bf16[1,2048,256]{2,1,0:T(8,128)(2,1)}, u32[]{:S(2)}) copy-start(bf16[1,2048,256]{2,1,0:T(8,128)(2,1)} %param.25) | copy-start | bytes 3145732
  39.0 2.7 %copy-start.3 = (f32[2048]{0:T(1024)S(1)}, f32[2048]{0:T(1024)}, u32[]{:S(2)}) copy-start(f32[2048]{0:T(1024)} %param.22) | copy-start | bytes 24580
  39.0 16.0 %all-to-all-start.3 = ((bf16[32,24,256]{2,1,0:T(8,128)(2,1)}), bf16[32,24,256]{2,1,0:T(8,128)(2,1)S(1)}, u32[]{:S(2)}, u32[]{:S(2)}) async-start(bf16[32,24,256]{2,1,0:T(8,128)(2,1)} %broadcast_in_dim.15), calls=%async_computation.3 | async-start | bytes 786432 | tf_op jit(solution)/shard_map/all_to_all | solution.py:97
  58.3 10.8 %all-to-all-start.4 = ((bf16[32,3,512]{2,1,0:T(4,128)(2,1)}), bf16[32,3,512]{2,1,0:T(4,128)(2,1)S(1)}, u32[]{:S(2)}, u32[]{:S(2)}) async-start(bf16[32,3,512]{2,1,0:T(4,128)(2,1)} %bitcast.13), calls=%async_computation.4 | async-start | bytes 262144 | tf_op jit(solution)/shard_map/all_to_all | solution.py:154
  60.8 0.7 copy-start.4
  61.5 0.7 copy-start.5

commit v3 on v2

--- a/solution.py
+++ b/solution.py
@@ -18,7 +18,7 @@
 
 def attend_body(length_ref, offset_ref, part_ref, token_ref, key_ref, value_ref, out_ref):
     batch, places, head_size = key_ref.shape
-    heads = offset_ref.shape[1]
+    heads = offset_ref.shape[0]
     rows = -(-batch * heads // 8) * 8
     wide = token_ref[...].astype(jnp.float32)
     norm = lax.rsqrt(jnp.mean(wide * wide, axis=-1, keepdims=True) + 1e-06)
@@ -36,7 +36,7 @@
         )
         lengths.append(jnp.full((heads, places), length_ref[b], jnp.int32))
         for h in range(heads):
-            offsets.append(jnp.full((1, places), offset_ref[0, h], jnp.float32))
+            offsets.append(jnp.full((1, places), offset_ref[h], jnp.float32))
     extra = rows - batch * heads
     if extra:
         scores.append(jnp.zeros((extra, places), jnp.float32))
@@ -89,7 +89,7 @@
         in_specs=[smem, smem, vmem, vmem, vmem, vmem],
         out_specs=vmem,
         name="attend",
-    )(lengths, offset.reshape(1, -1), parts, tokens, keys, values)
+    )(lengths, offset, parts, tokens, keys, values)
 
 
 def spread(block, axes, count):
@@ -122,6 +122,10 @@
     both = ("ep", "tp")
     columns = output_weight.shape[1]
 
+    out_weights = [output_weight] + [
+        lax.ppermute(output_weight, "tp", [(s, s ^ step) for s in range(tp_count)])
+        for step in range(1, tp_count)
+    ]
     feature_count = query_weight.shape[0]
     raw = lax.all_to_all(tokens, "ep", split_axis=1, concat_axis=0, tiled=True)
     gain = lax.dynamic_slice_in_dim(mixer_gain, ep_index * feature_count, feature_count, 0)
@@ -133,14 +137,17 @@
     batch_places = key_cache.shape[:2]
     keys = key_cache.reshape(*batch_places, -1)
     values = value_cache.reshape(*batch_places, -1)
-    outward = attend(parts, tokens, keys, values, seq_lengths, head_offset, ep_count)
-    inward = lax.all_to_all(outward, "ep", split_axis=0, concat_axis=0, tiled=True)
-    heads_out = inward.reshape(total, -1)
-    part = jnp.dot(heads_out, output_weight, preferred_element_type=jnp.float32)
-    part = part + jnp.where(tp_index == 0, raw.astype(jnp.float32), 0.0)
-    terms = spread(part.astype(jnp.bfloat16), both, ep_count * tp_count)
-    terms = terms.reshape(ep_count, tp_count, total, columns)
-    resid = jnp.sum(terms.astype(jnp.float32), axis=1).astype(jnp.bfloat16)
+    outward = attend(parts, tokens, keys, values, seq_lengths, head_offset, ep_count * tp_count)
+    inward = lax.all_to_all(outward, both, split_axis=0, concat_axis=0, tiled=True)
+    inward = inward.reshape(ep_count, tp_count, batch, -1)
+    summed = raw.astype(jnp.float32)
+    for step in range(tp_count):
+        quarter = lax.dynamic_index_in_dim(inward, tp_index ^ step, 1, keepdims=False)
+        part = jnp.dot(
+            quarter.reshape(total, -1), out_weights[step], preferred_element_type=jnp.float32
+        )
+        summed = summed + part.astype(jnp.bfloat16).astype(jnp.float32)
+    resid = spread(summed.astype(jnp.bfloat16), "ep", ep_count)
     resid = resid.transpose(1, 0, 2).reshape(total, width)
 
     normed2 = rms_norm(resid, expert_gain)

time: 70.4 us -> 66.6 us (0.946)
  blocking collectives: 9.96 us -> 0 us
  starting transfers between devices: 16.1 us -> 21.2 us
  local copies, waits for them, and re-layouts: 3.87 us -> 5.17 us
  matrix products: 3.45 us -> 2.72 us
    all_to_all x1 -> x0, blocking collectives: 9.96 us -> none  [local(): lax.all_to_all(partial_query, 'ep', split_axis=0, concat_axis=0, tiled=True)]
    all_to_all x1 -> x2, waiting for transfers between devices: 6.6 us -> 13.1 us  [the longest x1 8.17 us: local(): lax.all_to_all(outward, both, split_axis=0, concat_axis=0, tiled=True)]
    all_to_all x1, waiting for transfers between devices: 13.2 us -> 7.07 us  [spread(): return lax.all_to_all(wide, axes, split_axis=0, concat_axis=0, tiled=True)]
    all_to_all x1 -> x2, starting transfers between devices: 3.33 us -> 5.91 us  [the longest x1 3.35 us: local(): lax.all_to_all(partial_query, 'ep', split_axis=0, concat_axis=0, tiled=True)]
    ppermute x0 -> x3, starting transfers between devices: none -> 1.92 us  [local(): lax.ppermute(output_weight, 'tp', [(s, s ^ step) for s in range(tp_count)])]
    dot_general x1, matrix products: 1.96 us -> 0.73 us  [local(): jnp.dot(hidden, down_weight[0], preferred_element_type=jnp.float32)]
    unnamed x14 -> x19, local copies, waits for them, and re-layouts: 1.47 us -> 2.16 us
  transfers between devices with their start and end apart: 4 -> 8, of which waited for: 4 -> 5; matrix products, arithmetic and copies ran while one was open for 2% -> 3% of each run, Pallas kernels for 0% -> 4%
where the time goes in v3:
time: 66.6 us; the launch traced here: 66 us
  waiting for transfers between devices  32.6 us (49%)
  starting transfers between devices  21.2 us (32%)
  local copies, waits for them, and re-layouts  5.17 us (8%)
  Pallas kernels  2.88 us (4%)
  matrix products  2.72 us (4%)
  other arithmetic  1.19 us (2%)
    all_to_all x1, waiting for transfers between devices, local(): lax.all_to_all(outward, both, split_axis=0, concat_axis=0, tiled=True)  8.17 us
    all_to_all x1, starting transfers between devices, local(): raw = lax.all_to_all(tokens, 'ep', split_axis=1, concat_axis=0, tiled=True)  7.44 us
    all_to_all x1, waiting for transfers between devices, spread(): return lax.all_to_all(wide, axes, split_axis=0, concat_axis=0, tiled=True)  7.07 us
    all_to_all x1, waiting for transfers between devices, local(): lax.all_to_all(outgoing, both, split_axis=0, concat_axis=0, tiled=True)  6.65 us
    all_to_all x1, waiting for transfers between devices, local(): raw = lax.all_to_all(tokens, 'ep', split_axis=1, concat_axis=0, tiled=True)  5.82 us
    all_to_all x1, waiting for transfers between devices, local(): lax.all_to_all(partial_query, 'ep', split_axis=0, concat_axis=0, tiled=True)  4.9 us
    all_to_all x1, starting transfers between devices, spread(): return lax.all_to_all(wide, axes, split_axis=0, concat_axis=0, tiled=True)  3.36 us
    all_to_all x1, starting transfers between devices, local(): lax.all_to_all(partial_query, 'ep', split_axis=0, concat_axis=0, tiled=True)  3.35 us
  transfers between devices with their start and end apart: 8, of which 5 were waited for; matrix products, arithmetic and copies ran while one was open for 3% of the time, Pallas kernels for 4%

profile of v3, /device:TPU:0, one launch (start us, length us, event | category | flops | bytes accessed | tf_op | source)
XLA Modules:
  0.0 66.0 jit_solution(14042596532371338370)
XLA Ops:
  0.0 7.4 %all-to-all-start = ((bf16[3,8,256]{2,0,1:T(4,128)(2,1)}), bf16[3,8,256]{2,0,1:T(4,128)(2,1)S(1)}, u32[]{:S(2)}, u32[]{:S(2)}) async-start(bf16[3,8,256]{2,0,1:T(4,128)(2,1)} %bitcast.68), calls=%async_computation | async-start | bytes 32768 | tf_op jit(solution)/shard_map/all_to_all | solution.py:130
  7.4 0.8 %dynamic_slice.19 = f32[256]{0:T(256)S(1)} dynamic-slice(f32[2048]{0:T(1024)} %param.15, s32[]{:T(128)S(6)} %select_n.26), dynamic_slice_sizes={256} | dynamic-slice | bytes 2052 | tf_op jit(solution)/shard_map/dynamic_slice | solution.py:131
  8.2 5.8 %all-to-all-done = bf16[3,8,256]{2,0,1:T(4,128)(2,1)S(1)} async-done(((bf16[3,8,256]{2,0,1:T(4,128)(2,1)}), bf16[3,8,256]{2,0,1:T(4,128)(2,1)S(1)}, u32[]{:S(2)}, u32[]{:S(2)}) %all-to-all-start) | async-done | bytes 12320 | tf_op jit(solution)/shard_map/all_to_all | solution.py:130
  14.0 1.1 %fusion.15 = f32[8,3,512]{2,0,1:T(8,128)S(1)} fusion(bf16[256,512]{1,0:T(8,128)(2,1)} %param.16, bf16[8,3,256]{2,1,0:T(4,128)(2,1)S(1)} %fusion.27), kind=kOutput, calls=%fused_computation.20 | convolution fusion | flops 6291456 | bytes 323584 | tf_op jit(solution)/shard_map/dot_general | solution.py:133
  15.2 0.7 %copy.57 = f32[8,3,512]{2,1,0:T(4,128)} copy(f32[8,3,512]{2,0,1:T(8,128)S(1)} %fusion.15) | data formatting | bytes 98304 | tf_op jit(solution)/shard_map/dot_general | solution.py:133
  15.9 3.3 %all-to-all-start.1 = ((f32[8,3,512]{2,1,0:T(4,128)}), f32[8,3,512]{2,1,0:T(4,128)S(1)}, u32[]{:S(2)}, u32[]{:S(2)}) async-start(f32[8,3,512]{2,1,0:T(4,128)} %copy.57), calls=%async_computation.1 | async-start | bytes 131072 | tf_op jit(solution)/shard_map/all_to_all | solution.py:134
  19.3 1.6 %collective-permute-start.1 = (bf16[512,256]{1,0:T(8,128)(2,1)S(1)}, bf16[512,256]{1,0:T(8,128)(2,1)S(1)}, u32[]{:S(2)}, u32[]{:S(2)}) collective-permute-start(bf16[512,256]{1,0:T(8,128)(2,1)S(1)} %copy-done.4), channel_id=1, source_target_pairs={{0,2},{1,3},{2,0},{3,1},{4,6},{5,7},{6,4},{7,5},{8,10},{9,11},{10,... | collective-permute-start | bytes 786440 | tf_op jit(solution)/shard_map/ppermute | solution.py:126
  20.9 0.3 collective-permute-start
  21.1 4.9 %all-to-all-done.1.part_ref = f32[8,3,512]{2,1,0:T(4,128)S(1)} async-done(((f32[8,3,512]{2,1,0:T(4,128)}), f32[8,3,512]{2,1,0:T(4,128)S(1)}, u32[]{:S(2)}, u32[]{:S(2)}) %all-to-all-start.1) | async-done | bytes 49184 | tf_op jit(solution)/shard_map/all_to_all | solution.py:134
  26.1 0.6 copy-done.3
  26.7 2.9 %attend.1 = bf16[32,3,512]{2,1,0:T(4,128)(2,1)} custom-call(s32[3]{0:T(128)} %length_ref.1, f32[4]{0:T(128)} %offset_ref.1, f32[8,3,512]{2,1,0:T(4,128)} %copy-done.3, bf16[3,2048]{1,0:T(4,128)(2,1)} %token_ref.1, bf16[3,1024,128]{2,1,0:T(8,128)(2,1)} %bitcast.63, bf16[3,1024,128]{2,1,0:T(8,128)(2,1)} %bitcast.64), custom_call_target="tpu_custom_call" | custom-call | tf_op jit(solution)/shard_map/attend/pallas_call | solution.py:86
  29.6 2.6 %all-to-all-start.2 = ((bf16[32,3,512]{2,1,0:T(4,128)(2,1)}), bf16[32,3,512]{2,1,0:T(4,128)(2,1)S(1)}, u32[]{:S(2)}, u32[]{:S(2)}) async-start(bf16[32,3,512]{2,1,0:T(4,128)(2,1)} %attend.1), calls=%async_computation.2 | async-start | bytes 262144 | tf_op jit(solution)/shard_map/all_to_all | solution.py:141
  32.2 8.2 %all-to-all-done.2 = bf16[32,3,512]{2,1,0:T(4,128)(2,1)S(1)} async-done(((bf16[32,3,512]{2,1,0:T(4,128)(2,1)}), bf16[32,3,512]{2,1,0:T(4,128)(2,1)S(1)}, u32[]{:S(2)}, u32[]{:S(2)}) %all-to-all-start.2) | async-done | bytes 98336 | tf_op jit(solution)/shard_map/all_to_all | solution.py:141
  41.2 0.6 broadcast_in_dim.10
  41.9 3.4 %all-to-all-start.3 = ((bf16[8,24,256]{2,1,0:T(8,128)(2,1)}), bf16[8,24,256]{2,1,0:T(8,128)(2,1)S(1)}, u32[]{:S(2)}, u32[]{:S(2)}) async-start(bf16[8,24,256]{2,1,0:T(8,128)(2,1)} %broadcast_in_dim.10), calls=%async_computation.3 | async-start | bytes 196608 | tf_op jit(solution)/shard_map/all_to_all | solution.py:97
  45.3 7.1 %all-to-all-done.3 = bf16[8,24,256]{2,1,0:T(8,128)(2,1)S(1)} async-done(((bf16[8,24,256]{2,1,0:T(8,128)(2,1)}), bf16[8,24,256]{2,1,0:T(8,128)(2,1)S(1)}, u32[]{:S(2)}, u32[]{:S(2)}) %all-to-all-start.3) | async-done | bytes 98336 | tf_op jit(solution)/shard_map/all_to_all | solution.py:97
  52.6 0.2 fusion.13
  52.9 0.7 %convolution_convert_fusion = bf16[24,2048]{1,0:T(8,128)(2,1)S(1)} fusion(bf16[24,2048]{1,0:T(8,128)(2,1)S(1)} %bitcast.62, bf16[1,256,2048]{2,1,0:T(8,128)(2,1)S(1)} %copy-done, bf16[1,2048,256]{2,1,0:T(8,128)(2,1)S(1)} %copy-done.2, f32[24,256]{1,0:T(8,128)S(1)} %fusion.13), kind=kOutput, calls=%fused_computation | convolution fusion | flops 50417664 | bytes 2318336 | tf_op jit(solution)/shard_map/dot_general | solution.py:157
  53.7 0.7 %copy.69 = bf16[8,4,3,512]{3,2,1,0:T(4,128)(2,1)} copy(bf16[8,4,3,512]{3,1,2,0:T(4,128)(2,1)S(1)} %bitcast.66) | data formatting | bytes 196608 | tf_op jit(solution)/shard_map/reshape | solution.py:160
  54.4 2.6 %all-to-all-start.4 = ((bf16[32,3,512]{2,1,0:T(4,128)(2,1)}), bf16[32,3,512]{2,1,0:T(4,128)(2,1)S(1)}, u32[]{:S(2)}, u32[]{:S(2)}) async-start(bf16[32,3,512]{2,1,0:T(4,128)(2,1)} %bitcast.12), calls=%async_computation.4 | async-start | bytes 262144 | tf_op jit(solution)/shard_map/all_to_all | solution.py:161
  57.0 0.7 %copy-done.6 = s32[3,2]{0,1:T(2,128)S(1)} copy-done((s32[3,2]{0,1:T(2,128)S(1)}, s32[3,2]{0,1:T(2,128)}, u32[]{:S(2)}) %copy-start.6) | copy-done | bytes 48
  57.7 0.6 copy-done.7
  58.5 6.6 %all-to-all-done.4 = bf16[32,3,512]{2,1,0:T(4,128)(2,1)S(1)} async-done(((bf16[32,3,512]{2,1,0:T(4,128)(2,1)}), bf16[32,3,512]{2,1,0:T(4,128)(2,1)S(1)}, u32[]{:S(2)}, u32[]{:S(2)}) %all-to-all-start.4) | async-done | bytes 98336 | tf_op jit(solution)/shard_map/all_to_all | solution.py:161
  65.3 0.7 %add_convert_fusion = bf16[3,512]{1,0:T(4,128)(2,1)} fusion(f32[3,512]{1,0:T(4,128)S(1)} %multiply_reduce_fusion, bf16[24,2048]{1,0:T(8,128)(2,1)S(1)} %bitcast.67, s32[]{:T(128)S(6)} %select_n.31, s32[]{:T(128)S(6)} %select_n.32), kind=kLoop, calls=%fused_computation.45 | loop fusion | flops 4608 | bytes 12296 | tf_op jit(solution)/shard_map/convert_element_type | solution.py:170
  (41 shorter events, 1.7 us)
Async XLA Ops:
  0.0 52.9 %copy-start = (bf16[1,256,2048]{2,1,0:T(8,128)(2,1)S(1)}, bf16[1,256,2048]{2,1,0:T(8,128)(2,1)}, u32[]{:S(2)}) copy-start(bf16[1,256,2048]{2,1,0:T(8,128)(2,1)} %param.27) | copy-start | bytes 3145732
  0.0 14.0 %all-to-all-start = ((bf16[3,8,256]{2,0,1:T(4,128)(2,1)}), bf16[3,8,256]{2,0,1:T(4,128)(2,1)S(1)}, u32[]{:S(2)}, u32[]{:S(2)}) async-start(bf16[3,8,256]{2,0,1:T(4,128)(2,1)} %bitcast.68), calls=%async_computation | async-start | bytes 32768 | tf_op jit(solution)/shard_map/all_to_all | solution.py:130
  14.0 5.2 %copy-start.4 = (bf16[512,256]{1,0:T(8,128)(2,1)S(1)}, bf16[512,256]{1,0:T(8,128)(2,1)}, u32[]{:S(2)}) copy-start(bf16[512,256]{1,0:T(8,128)(2,1)} %param.21) | copy-start | bytes 786436
  15.9 10.2 %all-to-all-start.1 = ((f32[8,3,512]{2,1,0:T(4,128)}), f32[8,3,512]{2,1,0:T(4,128)S(1)}, u32[]{:S(2)}, u32[]{:S(2)}) async-start(f32[8,3,512]{2,1,0:T(4,128)} %copy.57), calls=%async_computation.1 | async-start | bytes 131072 | tf_op jit(solution)/shard_map/all_to_all | solution.py:134
  19.2 21.3 %collective-permute-start.2 = (bf16[512,256]{1,0:T(8,128)(2,1)S(1)}, bf16[512,256]{1,0:T(8,128)(2,1)S(1)}, u32[]{:S(2)}, u32[]{:S(2)}) collective-permute-start(bf16[512,256]{1,0:T(8,128)(2,1)S(1)} %copy-done.4), channel_id=1, source_target_pairs={{0,3},{1,2},{2,1},{3,0},{4,7},{5,6},{6,5},{7,4},{8,11},{9,10},{10,... | collective-permute-start | bytes 786440 | tf_op jit(solution)/shard_map/ppermute | solution.py:126
  19.3 21.3 %collective-permute-start.1 = (bf16[512,256]{1,0:T(8,128)(2,1)S(1)}, bf16[512,256]{1,0:T(8,128)(2,1)S(1)}, u32[]{:S(2)}, u32[]{:S(2)}) collective-permute-start(bf16[512,256]{1,0:T(8,128)(2,1)S(1)} %copy-done.4), channel_id=1, source_target_pairs={{0,2},{1,3},{2,0},{3,1},{4,6},{5,7},{6,4},{7,5},{8,10},{9,11},{10,... | collective-permute-start | bytes 786440 | tf_op jit(solution)/shard_map/ppermute | solution.py:126
  20.9 20.2 %collective-permute-start = (bf16[512,256]{1,0:T(8,128)(2,1)S(1)}, bf16[512,256]{1,0:T(8,128)(2,1)S(1)}, u32[]{:S(2)}, u32[]{:S(2)}) collective-permute-start(bf16[512,256]{1,0:T(8,128)(2,1)S(1)} %copy-done.4), channel_id=1, source_target_pairs={{0,1},{1,0},{2,3},{3,2},{4,5},{5,4},{6,7},{7,6},{8,9},{9,8},{10,11... | collective-permute-start | bytes 786440 | tf_op jit(solution)/shard_map/ppermute | solution.py:126
  26.1 0.6 copy-start.3
  29.6 10.8 %all-to-all-start.2 = ((bf16[32,3,512]{2,1,0:T(4,128)(2,1)}), bf16[32,3,512]{2,1,0:T(4,128)(2,1)S(1)}, u32[]{:S(2)}, u32[]{:S(2)}) async-start(bf16[32,3,512]{2,1,0:T(4,128)(2,1)} %attend.1), calls=%async_computation.2 | async-start | bytes 262144 | tf_op jit(solution)/shard_map/all_to_all | solution.py:141
  40.6 12.0 %copy-start.1 = (bf16[1,2048,256]{2,1,0:T(8,128)(2,1)S(1)}, bf16[1,2048,256]{2,1,0:T(8,128)(2,1)}, u32[]{:S(2)}) copy-start(bf16[1,2048,256]{2,1,0:T(8,128)(2,1)} %param.25) | copy-start | bytes 3145732
  41.0 4.2 %copy-start.5 = (f32[2048]{0:T(1024)S(1)}, f32[2048]{0:T(1024)}, u32[]{:S(2)}) copy-start(f32[2048]{0:T(1024)} %param.22) | copy-start | bytes 24580
  41.2 11.7 %copy-start.2 = (bf16[1,2048,256]{2,1,0:T(8,128)(2,1)S(1)}, bf16[1,2048,256]{2,1,0:T(8,128)(2,1)}, u32[]{:S(2)}) copy-start(bf16[1,2048,256]{2,1,0:T(8,128)(2,1)} %param.26) | copy-start | bytes 3145732
  41.9 10.5 %all-to-all-start.3 = ((bf16[8,24,256]{2,1,0:T(8,128)(2,1)}), bf16[8,24,256]{2,1,0:T(8,128)(2,1)S(1)}, u32[]{:S(2)}, u32[]{:S(2)}) async-start(bf16[8,24,256]{2,1,0:T(8,128)(2,1)} %broadcast_in_dim.10), calls=%async_computation.3 | async-start | bytes 196608 | tf_op jit(solution)/shard_map/all_to_all | solution.py:97
  54.4 10.8 %all-to-all-start.4 = ((bf16[32,3,512]{2,1,0:T(4,128)(2,1)}), bf16[32,3,512]{2,1,0:T(4,128)(2,1)S(1)}, u32[]{:S(2)}, u32[]{:S(2)}) async-start(bf16[32,3,512]{2,1,0:T(4,128)(2,1)} %bitcast.12), calls=%async_computation.4 | async-start | bytes 262144 | tf_op jit(solution)/shard_map/all_to_all | solution.py:161
  57.0 0.7 %copy-start.6 = (s32[3,2]{0,1:T(2,128)S(1)}, s32[3,2]{0,1:T(2,128)}, u32[]{:S(2)}) copy-start(s32[3,2]{0,1:T(2,128)} %param.23) | copy-start | bytes 76
  57.6 0.7 %copy-start.7 = (f32[3,2]{0,1:T(2,128)S(1)}, f32[3,2]{0,1:T(2,128)}, u32[]{:S(2)}) copy-start(f32[3,2]{0,1:T(2,128)} %param.24) | copy-start | bytes 76
